TPU v7x, 32 devices: a whole 2x2x4 slice. The times are simulated.
32 devices in a mesh: fs: 8 (over z, y), tp: 4 (over x, core).
Axes of the slice: x: 2, y: 2, z: 4, core: 2. Of those that a mesh axis runs over, the one named last changes fastest.
Arguments:
- prompt_tokens: bfloat16 [768, 4096], P('tp'), may hold values from -6 to 6
- norm_gain: float32 [4096], P('fs'), may hold values from 0.1 to 1.9
- gate_trained: float32 [4096, 11264], P('fs', 'tp'), may hold values from -0.09375 to 0.09375
- up_trained: float32 [4096, 11264], P('fs', 'tp'), may hold values from -0.09375 to 0.09375
- down_trained: float32 [11264, 4096], P('fs', 'tp'), may hold values from -0.078125 to 0.078125
Outputs:
- gate_serving: bfloat16 [4096, 11264], P(None, 'fs')
- up_serving: bfloat16 [4096, 11264], P(None, 'fs')
- down_serving: bfloat16 [11264, 4096], P('fs')
- mixed: bfloat16 [768, 4096], P('tp', 'fs')
All inputs are finite; a program needn't handle non-finite values.
Results may differ from a plain program's by a relative error of at most 0.0082.
Values may be sent and summed in bfloat16 or wider, within the bound.
A program may use at most 128 MiB of HBM per device.

v0:
```python
import jax
import jax.numpy as jnp
from jax import lax
from jax.sharding import PartitionSpec as P


def on_device(prompt_tokens, norm_gain, gate_trained, up_trained, down_trained):
    fs_count = lax.axis_size("fs")
    gate_cast = (gate_trained * norm_gain[:, None]).astype(jnp.bfloat16)
    up_cast = (up_trained * norm_gain[:, None]).astype(jnp.bfloat16)
    down_cast = down_trained.astype(jnp.bfloat16)
    down_serving = lax.all_gather(down_cast, "tp", axis=1, tiled=True)
    gate_part, up_part = (
        lax.all_to_all(gate_cast, "tp", split_axis=0, concat_axis=1, tiled=True),
        lax.all_to_all(up_cast, "tp", split_axis=0, concat_axis=1, tiled=True),
    )
    gate_mid, up_mid = (
        lax.all_to_all(gate_part, "fs", split_axis=1, concat_axis=0, tiled=True),
        lax.all_to_all(up_part, "fs", split_axis=1, concat_axis=0, tiled=True),
    )
    share = gate_mid.shape[0] // fs_count
    width = gate_mid.shape[1]
    gate_blocks, up_blocks = (
        lax.all_gather(gate_mid.reshape(fs_count, share, width), "tp", axis=1, tiled=True),
        lax.all_gather(up_mid.reshape(fs_count, share, width), "tp", axis=1, tiled=True),
    )
    gate_serving = gate_blocks.reshape(-1, width)
    up_serving = up_blocks.reshape(-1, width)
    tokens = prompt_tokens.astype(jnp.float32)
    scale = lax.rsqrt(jnp.mean(tokens * tokens, axis=-1, keepdims=True) + 1e-06)
    normed = (tokens * scale).astype(jnp.bfloat16)
    contract = (((0,), (1,)), ((), ()))
    gate_cols = lax.dot_general(gate_serving, normed, contract, preferred_element_type=jnp.float32)
    up_cols = lax.dot_general(up_serving, normed, contract, preferred_element_type=jnp.float32)
    hidden_cols = (jax.nn.silu(gate_cols) * up_cols).astype(jnp.bfloat16)
    summed = lax.psum_scatter(
        lax.dot_general(
            down_serving, hidden_cols, (((0,), (0,)), ((), ())), preferred_element_type=jnp.float32
        ),
        "fs",
        scatter_dimension=0,
        tiled=True,
    )
    mixed = summed.T.astype(jnp.bfloat16)
    return (gate_serving, up_serving, down_serving, mixed)


def solution(mesh):
    return jax.shard_map(
        on_device,
        mesh=mesh,
        in_specs=(P("tp", None), P("fs"), P("fs", "tp"), P("fs", "tp"), P("fs", "tp")),
        out_specs=(P(None, "fs"), P(None, "fs"), P("fs", None), P("tp", "fs")),
        check_vma=False,
    )
```

profile of v0, /device:TPU:0, one launch (start us, length us, event | category | flops | bytes accessed | tf_op | source)
XLA Modules:
  0.0 524.6 jit_solution(6554279546055345411)
XLA Ops:
  7.2 0.0 all-gather.4.cloned.1.call-start
  7.2 5.5 %multiply_convert_fusion = (bf16[512,2816]{1,0:T(8,128)(2,1)S(1)}, bf16[512,2816]{1,0:T(8,128)(2,1)S(1)}) fusion(f32[512,2816]{1,0:T(8,128)} %param.8, f32[512]{0:T(512)} %param.6, f32[512,2816]{1,0:T(8,128)} %param.7), kind=kLoop, calls=%fused_computation | loop fusion | flops 5767168 | bytes 17303552 | tf_op jit(solution)/shard_map/convert_element_type | solution.py:10
  12.7 38.2 %all_to_all.64 = bf16[4,128,2816]{2,1,0:T(8,128)(2,1)} all-to-all(bf16[4,128,2816]{2,1,0:T(8,128)(2,1)S(1)} %bitcast.18), channel_id=1, replica_groups=mesh['fs'=8,'tp'=4] {'tp'}, dimensions={0} | all-to-all | bytes 5767168 | tf_op jit(solution)/shard_map/all_to_all | solution.py:14
  51.0 4.5 copy.9
  55.5 71.4 %all_to_all.65 = bf16[128,8,1408]{0,2,1:T(8,128)(2,1)} all-to-all(bf16[128,8,1408]{0,2,1:T(8,128)(2,1)} %bitcast.26), channel_id=1, replica_groups=mesh['fs'=8,'tp'=4] {'fs'}, dimensions={1} | all-to-all | bytes 5767168 | tf_op jit(solution)/shard_map/all_to_all | solution.py:18
  126.9 0.0 all-gather.4.cloned.1.call-update
  126.9 0.0 all-gather.6.cloned.1.call-start
  127.0 64.5 %all_to_all.66 = bf16[4,128,2816]{2,1,0:T(8,128)(2,1)} all-to-all(bf16[4,128,2816]{2,1,0:T(8,128)(2,1)S(1)} %bitcast.17), channel_id=1, replica_groups=mesh['fs'=8,'tp'=4] {'tp'}, dimensions={0} | all-to-all | bytes 5767168 | tf_op jit(solution)/shard_map/all_to_all | solution.py:15
  191.5 3.3 copy.11
  194.8 67.9 %all_to_all.67 = bf16[128,8,1408]{0,2,1:T(8,128)(2,1)} all-to-all(bf16[128,8,1408]{0,2,1:T(8,128)(2,1)S(1)} %bitcast.28), channel_id=1, replica_groups=mesh['fs'=8,'tp'=4] {'fs'}, dimensions={1} | all-to-all | bytes 5767168 | tf_op jit(solution)/shard_map/all_to_all | solution.py:19
  262.7 0.0 all-gather.6.cloned.1.call-update
  262.8 0.0 all-gather.8.cloned.1.call-start
  262.8 4.7 convert_element_type.26
  267.5 0.0 copy-start
  267.5 0.0 all-gather.8.cloned.1.call-update
  267.5 0.0 reduce-scatter.2.cloned.1.call-start
  267.6 1.6 copy-done
  269.1 0.4 fusion
  269.5 0.0 all-gather.4.cloned.1.call-done
  269.6 16.0 %copy.10 = bf16[8,512,1408]{2,1,0:T(8,128)(2,1)} copy(bf16[8,512,1408]{1,2,0:T(8,128)(2,1)} %all-gather.4.cloned.1.call-done) | data formatting | bytes 23068672 | tf_op jit(solution)/shard_map/all_gather | solution.py:24
  285.6 53.0 %all-gather.6.cloned.1.call-done = bf16[8,512,1408]{1,2,0:T(8,128)(2,1)} async-done(((bf16[8,128,1408]{1,2,0:T(8,128)(2,1)}), bf16[8,512,1408]{1,2,0:T(8,128)(2,1)}) %all-gather.6.cloned.1.call-update) | async-done | bytes 11534352 | tf_op jit(solution)/shard_map/all_gather | solution.py:25
  338.5 16.0 %copy.12 = bf16[8,512,1408]{2,1,0:T(8,128)(2,1)} copy(bf16[8,512,1408]{1,2,0:T(8,128)(2,1)} %all-gather.6.cloned.1.call-done) | data formatting | bytes 23068672 | tf_op jit(solution)/shard_map/all_gather | solution.py:25
  354.5 7.2 %fusion.3 = f32[1408,192]{0,1:T(8,128)S(1)} fusion(bf16[4096,1408]{1,0:T(8,128)(2,1)} %bitcast.19, bf16[192,4096]{1,0:T(8,128)(2,1)S(1)} %copy-done, f32[192]{0:T(256)S(1)} %add_rsqrt_fusion), kind=kOutput, calls=%fused_computation.9 | convolution fusion | flops 2216951808 | bytes 14189312 | tf_op jit(solution)/shard_map/dot_general | solution.py:33
  361.8 55.1 %all-gather.8.cloned.1.call-done = bf16[1408,4096]{1,0:T(8,128)(2,1)} async-done(((bf16[1408,1024]{1,0:T(8,128)(2,1)}), bf16[1408,4096]{1,0:T(8,128)(2,1)}) %all-gather.8.cloned.1.call-update) | async-done | bytes 11534352 | tf_op jit(solution)/shard_map/all_gather | solution.py:12
  416.8 14.4 %convolution_bitcast_fusion = f32[4096,192]{0,1:T(8,128)} fusion(bf16[1408,4096]{1,0:T(8,128)(2,1)} %all-gather.8.cloned.1.call-done, bf16[4096,1408]{1,0:T(8,128)(2,1)} %bitcast.21, f32[1408,192]{0,1:T(8,128)S(1)} %fusion.3, bf16[192,4096]{1,0:T(8,128)(2,1)S(1)} %copy-done, f32[192]{0:T(256)S(1)} %add_rsqrt_fusion), kind=kOutput, calls=%fused_computation.2 | convolution fusion | flops 4433166336 | bytes 28869376 | tf_op jit(solution)/shard_map/dot_general | solution.py:37
  431.3 0.0 reduce-scatter.2.cloned.1.call-update
  431.3 75.0 %reduce-scatter.2.cloned.1.call-done = f32[512,192]{0,1:T(8,128)} async-done(((f32[4096,192]{0,1:T(8,128)}), f32[512,192]{0,1:T(8,128)}) %reduce-scatter.2.cloned.1.call-update) | async-done | bytes 393232 | tf_op jit(solution)/shard_map/reduce_scatter | solution.py:36
  506.3 1.7 convert_bitcast_fusion
  508.0 10.1 %copy.14 = bf16[1408,4096]{1,0:T(8,128)(2,1)} copy(bf16[1408,4096]{1,0:T(8,128)(2,1)} %all-gather.8.cloned.1.call-done) | data formatting | bytes 23068672
  (1 shorter events, 0.0 us)
Async XLA Ops:
  7.2 262.4 %all-gather.4.cloned.1.call-start = ((), (), s32[]{:S(2)}) async-start(), calls=%async_computation.5 | async-start | bytes 14417920 | tf_op jit(solution)/shard_map/all_gather | solution.py:24
  126.9 211.6 %all-gather.6.cloned.1.call-start = ((), (), s32[]{:S(2)}) async-start(), calls=%async_computation.6 | async-start | bytes 14417920 | tf_op jit(solution)/shard_map/all_gather | solution.py:25
  262.8 154.1 %all-gather.8.cloned.1.call-start = ((), (), s32[]{:S(2)}) async-start(), calls=%async_computation.7 | async-start | bytes 14417920 | tf_op jit(solution)/shard_map/all_gather | solution.py:12
  267.5 1.6 copy-start
  267.5 238.8 %reduce-scatter.2.cloned.1.call-start = ((), (), s32[]{:S(2)}) async-start(), calls=%async_computation.8 | async-start | bytes 3538944 | tf_op jit(solution)/shard_map/reduce_scatter | solution.py:36
Sparse Core Ops, SparseCore 0:
  127.1 102.4 all-gather.3
  262.9 75.5 all-gather.5
  340.7 76.1 all-gather.7
  431.4 74.8 reduce-scatter.1
where the time goes:
time: 526 us; the launch traced here: 525 us
  blocking collectives  242 us (46%)
  waiting for transfers between devices  183 us (35%)
  local copies, waits for them, and re-layouts  51.5 us (10%)
  matrix products  21.7 us (4%)
  between operations  13.8 us (3%)
  other arithmetic  12.3 us (2%)
    reduce_scatter x1, waiting for transfers between devices, on_device(): lax.psum_scatter(lax.dot_general(down_serving, hidden_cols, (((0,), (0,))...  75 us
    all_to_all x1, blocking collectives, on_device(): lax.all_to_all(gate_part, 'fs', split_axis=1, concat_axis=0, tiled=True)  71.4 us
    all_to_all x1, blocking collectives, on_device(): lax.all_to_all(up_part, 'fs', split_axis=1, concat_axis=0, tiled=True)  67.9 us
    all_to_all x1, blocking collectives, on_device(): lax.all_to_all(up_cast, 'tp', split_axis=0, concat_axis=1, tiled=True)  64.5 us
    all_gather x1, waiting for transfers between devices, on_device(): down_serving = lax.all_gather(down_cast, 'tp', axis=1, tiled=True)  55.1 us
    all_gather x1, waiting for transfers between devices, on_device(): lax.all_gather(up_mid.reshape(fs_count, share, width), 'tp', axis=1, tile...  53 us
    all_to_all x1, blocking collectives, on_device(): lax.all_to_all(gate_cast, 'tp', split_axis=0, concat_axis=1, tiled=True)  38.2 us
    all_gather x1, local copies, waits for them, and re-layouts, on_device(): lax.all_gather(up_mid.reshape(fs_count, share, width), 'tp', axis=1, tile...  16 us
  transfers between devices with their start and end apart: 4, of which 3 were waited for; matrix products, arithmetic and copies ran while one was open for 9% of the time, Pallas kernels for 0%

commit v1 on v0

--- a/solution.py
+++ b/solution.py
@@ -2,6 +2,22 @@
 import jax.numpy as jnp
 from jax import lax
 from jax.sharding import PartitionSpec as P
+
+
+def exchange_in_pairs(shard, axis, split, join):
+    ways, here = (lax.axis_size(axis), lax.axis_index(axis))
+    width = shard.shape[split] // ways
+    lengths = list(shard.shape)
+    lengths[split] = width
+    height = lengths[join]
+    lengths[join] = height * ways
+    full = jnp.zeros(lengths, shard.dtype)
+    for mask in range(ways):
+        part = lax.dynamic_slice_in_dim(shard, (here ^ mask) * width, width, axis=split)
+        if mask:
+            part = lax.ppermute(part, axis, [(d, d ^ mask) for d in range(ways)])
+        full = lax.dynamic_update_slice_in_dim(full, part, (here ^ mask) * height, axis=join)
+    return full
 
 
 def on_device(prompt_tokens, norm_gain, gate_trained, up_trained, down_trained):
@@ -15,7 +31,7 @@
         lax.all_to_all(up_cast, "tp", split_axis=0, concat_axis=1, tiled=True),
     )
     gate_mid, up_mid = (
-        lax.all_to_all(gate_part, "fs", split_axis=1, concat_axis=0, tiled=True),
+        exchange_in_pairs(gate_part, "fs", 1, 0),
         lax.all_to_all(up_part, "fs", split_axis=1, concat_axis=0, tiled=True),
     )
     share = gate_mid.shape[0] // fs_count

time: 526 us -> 542 us (1.030)
  blocking collectives: 242 us -> 137 us
  waiting for transfers between devices: 183 us -> 262 us
  local copies, waits for them, and re-layouts: 51.5 us -> 72.8 us
  starting transfers between devices: 0.16 us -> 17.9 us
    all_to_all x2 -> x0, blocking collectives: 110 us -> none  [the longest x1 71.4 us: on_device(): lax.all_to_all(gate_part, 'fs', split_axis=1, concat_axis=0, tiled=True)]
    all_to_all x0 -> x1, waiting for transfers between devices: none -> 34.7 us  [on_device(): lax.all_to_all(gate_cast, 'tp', split_axis=0, concat_axis=1, tiled=True)]
    ppermute x0 -> x7, waiting for transfers between devices: none -> 30.3 us  [exchange_in_pairs(): part = lax.ppermute(part, axis, [(d, d ^ mask) for d in range(ways)])]
    all_gather x1 -> x0, local copies, waits for them, and re-layouts: 16 us -> none  [on_device(): lax.all_gather(gate_mid.reshape(fs_count, share, width), 'tp', axis=1, ti...]
    ppermute x0 -> x7, starting transfers between devices: none -> 13 us  [exchange_in_pairs(): part = lax.ppermute(part, axis, [(d, d ^ mask) for d in range(ways)])]
    ppermute x0 -> x7, local copies, waits for them, and re-layouts: none -> 11.1 us  [exchange_in_pairs(): part = lax.ppermute(part, axis, [(d, d ^ mask) for d in range(ways)])]
    dynamic_update_slice x0 -> x8, local copies, waits for them, and re-layouts: none -> 10 us  [exchange_in_pairs(): lax.dynamic_update_slice_in_dim(full, part, (here ^ mask) * height, axis=...]
    unnamed x3 -> x4, local copies, waits for them, and re-layouts: 11.7 us -> 21.4 us
  transfers between devices with their start and end apart: 4 -> 12, of which waited for: 3 -> 7; matrix products, arithmetic and copies ran while one was open for 9% -> 10% of each run, Pallas kernels for 0% -> 0%
where the time goes in v1:
time: 542 us; the launch traced here: 541 us
  waiting for transfers between devices  262 us (48%)
  blocking collectives  137 us (25%)
  local copies, waits for them, and re-layouts  72.8 us (13%)
  matrix products  23.2 us (4%)
  starting transfers between devices  17.9 us (3%)
  between operations  13.9 us (3%)
  other arithmetic  13.8 us (3%)
    all_to_all x1, blocking collectives, on_device(): lax.all_to_all(up_part, 'fs', split_axis=1, concat_axis=0, tiled=True)  76.9 us
    reduce_scatter x1, waiting for transfers between devices, on_device(): lax.psum_scatter(lax.dot_general(down_serving, hidden_cols, (((0,), (0,))...  74.9 us
    all_gather x1, waiting for transfers between devices, on_device(): down_serving = lax.all_gather(down_cast, 'tp', axis=1, tiled=True)  62.3 us
    all_gather x1, waiting for transfers between devices, on_device(): lax.all_gather(up_mid.reshape(fs_count, share, width), 'tp', axis=1, tile...  60.2 us
    all_to_all x1, blocking collectives, on_device(): lax.all_to_all(up_cast, 'tp', split_axis=0, concat_axis=1, tiled=True)  59.9 us
    all_to_all x1, waiting for transfers between devices, on_device(): lax.all_to_all(gate_cast, 'tp', split_axis=0, concat_axis=1, tiled=True)  34.7 us
    ppermute x7, waiting for transfers between devices, exchange_in_pairs(): part = lax.ppermute(part, axis, [(d, d ^ mask) for d in range(ways)])  30.3 us
    unnamed x4, local copies, waits for them, and re-layouts  21.4 us
  transfers between devices with their start and end apart: 12, of which 7 were waited for; matrix products, arithmetic and copies ran while one was open for 10% of the time, Pallas kernels for 0%

profile of v1, /device:TPU:0, one launch (start us, length us, event | category | flops | bytes accessed | tf_op | source)
XLA Modules:
  0.0 540.9 jit_solution(3666838855310674838)
XLA Ops:
  7.2 7.1 %multiply_convert_fusion = (bf16[512,2816]{1,0:T(8,128)(2,1)S(1)}, bf16[512,2816]{1,0:T(8,128)(2,1)}) fusion(f32[512,2816]{1,0:T(8,128)} %param.8, f32[512]{0:T(512)} %param.6, f32[512,2816]{1,0:T(8,128)} %param.7), kind=kLoop, calls=%fused_computation | loop fusion | flops 5767168 | bytes 17303552 | tf_op jit(solution)/shard_map/convert_element_type | solution.py:26
  14.2 4.6 all-to-all-start
  19.0 34.7 %all-to-all-done = bf16[4,128,2816]{2,1,0:T(8,128)(2,1)} async-done(((bf16[4,128,2816]{2,1,0:T(8,128)(2,1)}), bf16[4,128,2816]{2,1,0:T(8,128)(2,1)}, u32[]{:S(2)}, u32[]{:S(2)}) %all-to-all-start) | async-done | bytes 2883616 | tf_op jit(solution)/shard_map/all_to_all | solution.py:30
  53.7 4.5 copy.9
  58.2 3.3 constant_dynamic-slice_fusion
  61.6 2.4 collective-permute-start
  63.9 1.6 collective-permute-start.1
  65.5 3.0 collective-permute-start.3
  68.5 1.2 copy.10
  69.7 1.4 collective-permute-start.4
  71.0 1.8 broadcast_in_dim.2
  72.8 0.8 constant_dynamic-update-slice_fusion.7
  73.6 3.6 collective-permute-start.5
  77.2 1.2 copy.11
  78.3 11.5 %collective-permute-done.1 = bf16[128,1408]{0,1:T(8,128)(2,1)} collective-permute-done((bf16[128,1408]{0,1:T(8,128)(2,1)}, bf16[128,1408]{0,1:T(8,128)(2,1)}, u32[]{:S(2)}, u32[]{:S(2)}) %collective-permute-start.1) | collective-permute-done | bytes 360480 | tf_op jit(solution)/shard_map/ppermute | solution.py:18
  89.9 1.1 collective-permute-start.6
  91.0 1.9 copy.12
  92.9 2.1 collective-permute-done.2
  95.0 1.9 copy.13
  96.9 1.9 copy.14
  98.8 0.8 constant_dynamic-update-slice_fusion.6
  99.6 1.7 constant_dynamic-update-slice_fusion.5
  101.3 16.6 %collective-permute-done.4 = bf16[128,1408]{0,1:T(8,128)(2,1)} collective-permute-done((bf16[128,1408]{0,1:T(8,128)(2,1)}, bf16[128,1408]{0,1:T(8,128)(2,1)}, u32[]{:S(2)}, u32[]{:S(2)}) %collective-permute-start.4) | collective-permute-done | bytes 360480 | tf_op jit(solution)/shard_map/ppermute | solution.py:18
  118.0 1.2 copy.15
  119.1 1.8 constant_dynamic-update-slice_fusion.4
  120.9 1.7 constant_dynamic-update-slice_fusion.3
  122.6 1.9 copy.16
  124.5 0.8 constant_dynamic-update-slice_fusion.2
  125.3 1.7 constant_dynamic-update-slice_fusion.1
  127.0 1.2 copy.17
  128.2 0.8 constant_dynamic-update-slice_fusion
  129.0 0.0 all-gather.6.cloned.1.call-start
  129.1 59.9 %all_to_all.51 = bf16[4,128,2816]{2,1,0:T(8,128)(2,1)} all-to-all(bf16[4,128,2816]{2,1,0:T(8,128)(2,1)S(1)} %bitcast.17), channel_id=1, replica_groups=mesh['fs'=8,'tp'=4] {'tp'}, dimensions={0} | all-to-all | bytes 5767168 | tf_op jit(solution)/shard_map/all_to_all | solution.py:31
  189.0 3.3 copy.18
  192.4 76.9 %all_to_all.52 = bf16[128,8,1408]{0,2,1:T(8,128)(2,1)} all-to-all(bf16[128,8,1408]{0,2,1:T(8,128)(2,1)S(1)} %bitcast.26), channel_id=1, replica_groups=mesh['fs'=8,'tp'=4] {'fs'}, dimensions={1} | all-to-all | bytes 5767168 | tf_op jit(solution)/shard_map/all_to_all | solution.py:35
  269.3 4.7 convert_element_type.26
  274.0 0.2 reduce-scatter.2.cloned.1.call-start
  274.3 1.4 copy-done
  275.7 0.4 fusion
  276.1 8.7 %fusion.3 = f32[1408,192]{0,1:T(8,128)S(1)} fusion(bf16[4096,1408]{1,0:T(8,128)(2,1)} %bitcast.19, bf16[192,4096]{1,0:T(8,128)(2,1)S(1)} %copy-done, f32[192]{0:T(256)S(1)} %add_rsqrt_fusion), kind=kOutput, calls=%fused_computation.9 | convolution fusion | flops 2216951808 | bytes 14189312 | tf_op jit(solution)/shard_map/dot_general | solution.py:49
  284.8 60.2 %all-gather.6.cloned.1.call-done = bf16[8,512,1408]{1,2,0:T(8,128)(2,1)} async-done(((bf16[8,128,1408]{1,2,0:T(8,128)(2,1)}), bf16[8,512,1408]{1,2,0:T(8,128)(2,1)}) %all-gather.6.cloned.1.call-update) | async-done | bytes 11534352 | tf_op jit(solution)/shard_map/all_gather | solution.py:41
  345.0 16.0 %copy.19 = bf16[8,512,1408]{2,1,0:T(8,128)(2,1)} copy(bf16[8,512,1408]{1,2,0:T(8,128)(2,1)} %all-gather.6.cloned.1.call-done) | data formatting | bytes 23068672 | tf_op jit(solution)/shard_map/all_gather | solution.py:41
  361.1 62.3 %all-gather.8.cloned.1.call-done = bf16[1408,4096]{1,0:T(8,128)(2,1)} async-done(((bf16[1408,1024]{1,0:T(8,128)(2,1)}), bf16[1408,4096]{1,0:T(8,128)(2,1)}) %all-gather.8.cloned.1.call-update) | async-done | bytes 11534352 | tf_op jit(solution)/shard_map/all_gather | solution.py:28
  423.4 14.4 %convolution_bitcast_fusion = f32[4096,192]{0,1:T(8,128)} fusion(bf16[1408,4096]{1,0:T(8,128)(2,1)} %all-gather.8.cloned.1.call-done, bf16[4096,1408]{1,0:T(8,128)(2,1)} %bitcast.21, f32[1408,192]{0,1:T(8,128)S(1)} %fusion.3, bf16[192,4096]{1,0:T(8,128)(2,1)S(1)} %copy-done, f32[192]{0:T(256)S(1)} %add_rsqrt_fusion), kind=kOutput, calls=%fused_computation.2 | convolution fusion | flops 4433166336 | bytes 28869376 | tf_op jit(solution)/shard_map/dot_general | solution.py:53
  437.8 74.9 %reduce-scatter.2.cloned.1.call-done = f32[512,192]{0,1:T(8,128)} async-done(((f32[4096,192]{0,1:T(8,128)}), f32[512,192]{0,1:T(8,128)}) %reduce-scatter.2.cloned.1.call-update) | async-done | bytes 393232 | tf_op jit(solution)/shard_map/reduce_scatter | solution.py:52
  512.7 1.7 convert_bitcast_fusion
  514.4 9.9 %copy.30 = bf16[4096,1408]{1,0:T(8,128)(2,1)} copy(bf16[4096,1408]{1,0:T(8,128)(2,1)} %bitcast.20) | data formatting | bytes 23068672
  524.3 10.1 %copy.31 = bf16[1408,4096]{1,0:T(8,128)(2,1)} copy(bf16[1408,4096]{1,0:T(8,128)(2,1)} %all-gather.8.cloned.1.call-done) | data formatting | bytes 23068672
  (14 shorter events, 0.2 us)
Async XLA Ops:
  14.2 39.4 %all-to-all-start = ((bf16[4,128,2816]{2,1,0:T(8,128)(2,1)}), bf16[4,128,2816]{2,1,0:T(8,128)(2,1)}, u32[]{:S(2)}, u32[]{:S(2)}) async-start(bf16[4,128,2816]{2,1,0:T(8,128)(2,1)} %bitcast.18), calls=%async_computation | async-start | bytes 5767168 | tf_op jit(solution)/shard_map/all_to_all | solution.py:30
  18.9 257.2 %all-gather.4.cloned.1.call-start = ((), (), s32[]{:S(2)}) async-start(), calls=%async_computation.4 | async-start | bytes 14417920 | tf_op jit(solution)/shard_map/all_gather | solution.py:40
  61.6 12.0 %collective-permute-start = (bf16[128,1408]{0,1:T(8,128)(2,1)}, bf16[128,1408]{0,1:T(8,128)(2,1)}, u32[]{:S(2)}, u32[]{:S(2)}) collective-permute-start(bf16[128,1408]{0,1:T(8,128)(2,1)} %get-tuple-element.10), channel_id=1, source_target_pairs={{0,4},{4,0},{8,12},{12,8},{16,20},{20,16},{24,28},{28,24},{1,5},{5... | collective-permute-start | bytes 1081352 | tf_op jit(solution)/shard_map/ppermute | solution.py:18
  63.9 26.0 %collective-permute-start.1 = (bf16[128,1408]{0,1:T(8,128)(2,1)}, bf16[128,1408]{0,1:T(8,128)(2,1)}, u32[]{:S(2)}, u32[]{:S(2)}) collective-permute-start(bf16[128,1408]{0,1:T(8,128)(2,1)} %get-tuple-element.9), channel_id=1, source_target_pairs={{0,8},{4,12},{8,0},{12,4},{16,24},{20,28},{24,16},{28,20},{1,9},{5... | collective-permute-start | bytes 1081352 | tf_op jit(solution)/shard_map/ppermute | solution.py:18
  65.5 29.5 %collective-permute-start.2 = (bf16[128,1408]{0,1:T(8,128)(2,1)}, bf16[128,1408]{0,1:T(8,128)(2,1)}, u32[]{:S(2)}, u32[]{:S(2)}) collective-permute-start(bf16[128,1408]{0,1:T(8,128)(2,1)} %get-tuple-element.8), channel_id=1, source_target_pairs={{0,12},{4,8},{8,4},{12,0},{16,28},{20,24},{24,20},{28,16},{1,13},{... | collective-permute-start | bytes 1081352 | tf_op jit(solution)/shard_map/ppermute | solution.py:18
  65.5 31.4 %collective-permute-start.3 = (bf16[128,1408]{0,1:T(8,128)(2,1)}, bf16[128,1408]{0,1:T(8,128)(2,1)}, u32[]{:S(2)}, u32[]{:S(2)}) collective-permute-start(bf16[128,1408]{0,1:T(8,128)(2,1)} %get-tuple-element.7), channel_id=1, source_target_pairs={{0,16},{4,20},{8,24},{12,28},{16,0},{20,4},{24,8},{28,12},{1,17},{... | collective-permute-start | bytes 1081352 | tf_op jit(solution)/shard_map/ppermute | solution.py:18
  69.7 48.3 %collective-permute-start.4 = (bf16[128,1408]{0,1:T(8,128)(2,1)}, bf16[128,1408]{0,1:T(8,128)(2,1)}, u32[]{:S(2)}, u32[]{:S(2)}) collective-permute-start(bf16[128,1408]{0,1:T(8,128)(2,1)} %get-tuple-element.6), channel_id=1, source_target_pairs={{0,20},{4,16},{8,28},{12,24},{16,4},{20,0},{24,12},{28,8},{1,21},{... | collective-permute-start | bytes 1081352 | tf_op jit(solution)/shard_map/ppermute | solution.py:18
  73.6 49.1 %collective-permute-start.5 = (bf16[128,1408]{0,1:T(8,128)(2,1)}, bf16[128,1408]{0,1:T(8,128)(2,1)}, u32[]{:S(2)}, u32[]{:S(2)}) collective-permute-start(bf16[128,1408]{0,1:T(8,128)(2,1)} %get-tuple-element.5), channel_id=1, source_target_pairs={{0,24},{4,28},{8,16},{12,20},{16,8},{20,12},{24,0},{28,4},{1,25},{... | collective-permute-start | bytes 1081352 | tf_op jit(solution)/shard_map/ppermute | solution.py:18
  89.9 37.2 %collective-permute-start.6 = (bf16[128,1408]{0,1:T(8,128)(2,1)}, bf16[128,1408]{0,1:T(8,128)(2,1)}, u32[]{:S(2)}, u32[]{:S(2)}) collective-permute-start(bf16[128,1408]{0,1:T(8,128)(2,1)} %get-tuple-element.4), channel_id=1, source_target_pairs={{0,28},{4,24},{8,20},{12,16},{16,12},{20,8},{24,4},{28,0},{1,29},{... | collective-permute-start | bytes 1081352 | tf_op jit(solution)/shard_map/ppermute | solution.py:18
  129.0 216.0 %all-gather.6.cloned.1.call-start = ((), (), s32[]{:S(2)}) async-start(), calls=%async_computation.5 | async-start | bytes 14417920 | tf_op jit(solution)/shard_map/all_gather | solution.py:41
  269.3 154.1 %all-gather.8.cloned.1.call-start = ((), (), s32[]{:S(2)}) async-start(), calls=%async_computation.6 | async-start | bytes 14417920 | tf_op jit(solution)/shard_map/all_gather | solution.py:28
  274.0 1.6 copy-start
  274.0 238.7 %reduce-scatter.2.cloned.1.call-start = ((), (), s32[]{:S(2)}) async-start(), calls=%async_computation.7 | async-start | bytes 3538944 | tf_op jit(solution)/shard_map/reduce_scatter | solution.py:52
Sparse Core Ops, SparseCore 0:
  129.1 100.9 all-gather.3
  269.4 75.5 all-gather.5
  347.2 76.1 all-gather.7
  437.9 74.7 reduce-scatter.1
